TPU v7x, 32 devices: a whole 2x2x4 slice. The times are simulated.
32 devices in a mesh: sp: 8 (over z, core), tp: 4 (over y, x).
Axes of the slice: x: 2, y: 2, z: 4, core: 2. Of those that a mesh axis runs over, the one named last changes fastest.
Arguments:
- prompt: bfloat16 [8, 2048, 2048], P('tp', 'sp'), may hold values from -6 to 6
- input_gain: float32 [2048], replicated, may hold values from 0.1 to 1.9
- key_weight: bfloat16 [1024, 2048], P('tp'), may hold values from -0.125 to 0.125
- value_weight: bfloat16 [1024, 2048], P('tp'), may hold values from -0.125 to 0.125
- key_gain: float32 [64], replicated, may hold values from 0.1 to 1.9
- queries: bfloat16 [8, 2, 1024], P('sp', None, 'tp'), may hold values from -6 to 6
- score_bias: float32 [2, 16], replicated, may hold values from -9 to -2
Outputs:
- keys: bfloat16 [8, 1024, 2048], P('sp', 'tp')
- values: bfloat16 [8, 1024, 2048], P('sp', 'tp')
- first_read: bfloat16 [8, 2, 1024], P('sp', None, 'tp')
All inputs are finite; a program needn't handle non-finite values.
Results may differ from a plain program's by a relative error of at most 0.01.
Values may be sent and summed in bfloat16 or wider, within the bound.
A program may use at most 64 MiB of HBM per device.

v0:
```python
import functools
import math

import jax
import jax.numpy as jnp
from jax import lax
from jax.experimental import pallas as pl
from jax.experimental.pallas import tpu as pltpu
from jax.sharding import PartitionSpec as P

HEAD = 64
LANES = 128
CORES = 2
NORM_ROWS = 16
W_CHUNKS = 4

epsilon = 1e-06
MESH = pl.DeviceIdType.MESH


def produce(
    dims, prompt, gain, key_w, value_w, key_gain, cache,
    x, xn, w, out, relay, gain_column,
    x_in, w_in, x_send, x_recv, w_send, w_recv, f_send, f_recv, h_send, h_recv, o_send, o_recv,
):
    sp, tp, A, B, R, halves, cols, width = dims
    s, t = lax.axis_index("sp"), lax.axis_index("tp")
    yb, xa = t // A, t % A
    core = s % CORES
    partner = s + 1 - 2 * core
    seqs = R // halves
    w_rows = cols // W_CHUNKS

    def local_x(i):
        return pltpu.make_async_copy(prompt.at[i], x.at[i], x_in.at[i])

    def local_w(k):
        return pltpu.make_async_copy((key_w, value_w)[k], w.at[0, k], w_in.at[k])

    for k in range(2):
        local_w(k).start()
    for i in range(R):
        local_x(i).start()

    def row_peer(db):
        return ((yb + db) % B) * A + xa

    def column_peer(da):
        return yb * A + (xa + da) % A

    barrier = pltpu.get_barrier_semaphore()

    def greet(k, _):
        other = lax.rem(s + k, sp)
        pl.semaphore_signal(barrier, inc=1, device_id={"sp": other, "tp": t}, device_id_type=MESH)
        return 0

    lax.fori_loop(1, sp, greet, 0)
    for da in range(1, A):
        pl.semaphore_signal(barrier, inc=1, device_id={"sp": s, "tp": column_peer(da)}, device_id_type=MESH)
    for db in range(1, B):
        pl.semaphore_signal(barrier, inc=1, device_id={"sp": s, "tp": row_peer(db)}, device_id_type=MESH)
    pl.semaphore_wait(barrier, sp - 1 + A - 1 + B - 1)

    def send_w(da, k):
        rows = pl.ds(k * w_rows, w_rows)
        return pltpu.make_async_remote_copy(
            src_ref=w.at[0, core, rows], dst_ref=w.at[da, core, rows],
            send_sem=w_send.at[da - 1, k], recv_sem=w_recv.at[da - 1, k],
            device_id={"sp": s, "tp": column_peer(da)}, device_id_type=MESH,
        )

    def forward_w(da, k):
        rows = pl.ds(k * w_rows, w_rows)
        return pltpu.make_async_remote_copy(
            src_ref=w.at[da, core, rows], dst_ref=w.at[da, core, rows],
            send_sem=f_send.at[da - 1, k], recv_sem=f_recv.at[da - 1, k],
            device_id={"sp": partner, "tp": t}, device_id_type=MESH,
        )

    def arrived_w(da, k):
        rows = pl.ds(k * w_rows, w_rows)
        return pltpu.make_async_remote_copy(
            src_ref=w.at[da, 1 - core, rows], dst_ref=w.at[da, 1 - core, rows],
            send_sem=f_send.at[da - 1, k], recv_sem=f_recv.at[da - 1, k],
            device_id={"sp": partner, "tp": t}, device_id_type=MESH,
        )

    def send_x(db, i):
        return pltpu.make_async_remote_copy(
            src_ref=x.at[i], dst_ref=x.at[db * R + i],
            send_sem=x_send.at[(db - 1) * R + i], recv_sem=x_recv.at[(db - 1) * R + i],
            device_id={"sp": s, "tp": row_peer(db)}, device_id_type=MESH,
        )

    for k in range(2):
        local_w(k).wait()
    for k in range(W_CHUNKS):
        for da in range(1, A):
            send_w(da, k).start()
    for i in range(R):
        local_x(i).wait()
        for db in range(1, B):
            send_x(db, i).start()

    def normalise(r):
        def rows(k, _):
            here = pl.ds(pl.multiple_of(k * NORM_ROWS, NORM_ROWS), NORM_ROWS)
            flat = x[r, here, :].astype(jnp.float32)
            scale = lax.rsqrt(jnp.mean(flat * flat, axis=-1, keepdims=True) + epsilon)
            xn[r, here, :] = (flat * scale * gain[...]).astype(jnp.bfloat16)
            return 0

        lax.fori_loop(0, LANES // NORM_ROWS, rows, 0)

    eye = lax.broadcasted_iota(jnp.int32, (HEAD, HEAD), 0) == lax.broadcasted_iota(jnp.int32, (HEAD, HEAD), 1)
    gain_column[...] = jnp.broadcast_to(
        jnp.sum(jnp.where(eye, key_gain[...], 0.0), axis=1, keepdims=True), (HEAD, LANES)
    )

    class Home:
        def __init__(self, r, da):
            db, i = r // R, r % R
            j, half = i // halves, i % halves
            rows_of = ((yb + B - db) % B) * A + (xa + da) % A
            seq = rows_of * seqs + j
            slot = r * A + da
            index = s * halves + half
            place = cache.at[:, :, pl.ds(pl.multiple_of(index * LANES, LANES), LANES)]
            block = out.at[r, 0] if isinstance(da, int) and da == 0 else relay.at[r, da - 1]
            self.here = seq == s
            self.remote = pltpu.make_async_remote_copy(
                src_ref=block, dst_ref=place, send_sem=o_send.at[slot], recv_sem=o_recv.at[index],
                device_id={"sp": seq, "tp": t}, device_id_type=MESH,
            )
            self.block, self.place, self.sem = block, place, o_recv.at[index]

        def start(self):
            @pl.when(self.here)
            def _():
                pltpu.make_async_copy(self.block, self.place, self.sem).start()

            @pl.when(jnp.logical_not(self.here))
            def _():
                self.remote.start()

        def wait_send(self):
            @pl.when(jnp.logical_not(self.here))
            def _():
                self.remote.wait_send()

    def hop(r, da):
        return pltpu.make_async_remote_copy(
            src_ref=out.at[r, da], dst_ref=relay.at[r, da - 1],
            send_sem=h_send.at[r, da - 1], recv_sem=h_recv.at[r, da - 1],
            device_id={"sp": s, "tp": yb * A + (xa + A - da) % A}, device_id_type=MESH,
        )

    def project(r, da):
        rows = xn[r]
        contract = (((1,), (1,)), ((), ()))
        raw = lax.dot_general(w[da, 0], rows, contract, preferred_element_type=jnp.float32)
        raw = raw.reshape(cols // HEAD, HEAD, LANES)
        scale = lax.rsqrt(jnp.mean(raw * raw, axis=1, keepdims=True) + epsilon)
        keys = raw * scale * gain_column[...][None]
        out[r, da, 0] = keys.reshape(cols, LANES).astype(jnp.bfloat16)
        out[r, da, 1] = lax.dot_general(
            w[da, 1], rows, contract, preferred_element_type=jnp.float32
        ).astype(jnp.bfloat16)

    def keep(r):
        project(r, 0)
        Home(r, 0).start()

    def give(r):
        def one(da, _):
            project(r, da)
            hop(r, da).start()
            return 0

        lax.fori_loop(1, A, one, 0)

    def pass_on(r):
        for da in range(1, A):
            hop(r, da).wait_recv()
            Home(r, da).start()

    def own_first(r, _):
        normalise(r)
        keep(r)
        return 0

    lax.fori_loop(0, R, own_first, 0)

    def take(n):
        i, db = n // (B - 1), 1 + n % (B - 1)
        send_x(db, i).wait_recv()
        r = db * R + i
        normalise(r)
        keep(r)
        return r

    N = R * (B - 1)
    theirs = [(1 + n % (B - 1)) * R + n // (B - 1) for n in range(N)]
    early = N // 2
    taken = 0
    for k in range(W_CHUNKS):
        for da in range(1, A):
            send_w(da, k).wait_recv()
            forward_w(da, k).start()
        while taken < early * (k + 1) // W_CHUNKS:
            take(taken)
            taken += 1
    for k in range(W_CHUNKS):
        for da in range(1, A):
            arrived_w(da, k).wait_recv()

    order = []
    for n in range(max(early, R)):
        order += theirs[n : n + 1] if n < early else []
        order += [n] if n < R else []
    order += theirs[early:]
    given, passed = 0, 0
    for r in order[: early + R]:
        give(r)
        given += 1
        if given > early:
            pass_on(order[passed])
            passed += 1
    for n in range(early, N):
        give(take(n))
        given += 1
        while passed < min(R + 2 * (n - early + 1), given if n == N - 1 else given - 1):
            pass_on(order[passed])
            passed += 1
    while passed < len(order):
        pass_on(order[passed])
        passed += 1

    for k in range(W_CHUNKS):
        for da in range(1, A):
            send_w(da, k).wait_send()
            forward_w(da, k).wait_send()
    for i in range(R):
        for db in range(1, B):
            send_x(db, i).wait_send()

    for r in range(B * R):
        for da in range(A):
            Home(r, da).wait_send()
            if da:
                hop(r, da).wait_send()

    def landed(n, _):
        place = cache.at[:, :, pl.ds(pl.multiple_of(n * LANES, LANES), LANES)]
        pltpu.make_async_copy(out.at[0, 0], place, o_recv.at[n]).wait()
        return 0

    lax.fori_loop(0, sp * halves, landed, 0)


def read(dims, queries, bias, cache, keys_out, values_out, first_out, keys, values, sems):
    group, heads, cols, length = dims
    rows = group * heads
    t = lax.axis_index("tp")
    in_k = pltpu.make_async_copy(cache.at[0], keys, sems.at[0])
    in_v = pltpu.make_async_copy(cache.at[1], values, sems.at[1])
    out_k = pltpu.make_async_copy(keys, keys_out.at[0], sems.at[2])
    out_v = pltpu.make_async_copy(values, values_out.at[0], sems.at[3])
    in_k.start()
    in_v.start()

    def spread(ref_value):
        n = ref_value.shape[1]
        parts = [jnp.broadcast_to(ref_value[g : g + 1], (heads, n)) for g in range(group)]
        return jnp.concatenate(parts, axis=0)

    row_head = lax.broadcasted_iota(jnp.int32, (rows, cols), 0) % heads
    own = (lax.broadcasted_iota(jnp.int32, (rows, cols), 1) // HEAD) == row_head
    query = jnp.where(own, spread(queries[...].astype(jnp.float32)), 0.0).astype(jnp.bfloat16)
    offsets = spread(bias[...])
    at = lax.broadcasted_iota(jnp.int32, offsets.shape, 1)
    mine = at == t * heads + lax.broadcasted_iota(jnp.int32, offsets.shape, 0) % heads
    offset = jnp.sum(jnp.where(mine, offsets, 0.0), axis=1, keepdims=True)

    in_k.wait()
    out_k.start()
    scores = jnp.dot(query, keys[...], preferred_element_type=jnp.float32)
    scores = scores / math.sqrt(HEAD) + offset
    soft = jnp.log1p(jnp.exp(-jnp.abs(scores)))
    log_break = jnp.minimum(scores, 0.0) - soft
    log_keep = jnp.minimum(-scores, 0.0) - soft
    lane = lax.broadcasted_iota(jnp.int32, (rows, length), 1)

    def ahead(v, k):
        return jnp.where(lane < length - k, pltpu.roll(v, length - k, 1), 0.0)

    later = ahead(log_keep, 1)
    k = 1
    while k < length:
        later = later + ahead(later, k)
        k *= 2
    weights = jnp.exp(log_break + later).astype(jnp.bfloat16)
    in_v.wait()
    out_v.start()
    taken = lax.dot_general(
        weights, values[...], (((1,), (1,)), ((), ())), preferred_element_type=jnp.float32
    )
    taken = jnp.where(own, taken, 0.0)
    for g in range(group):
        first_out[g : g + 1, :] = jnp.sum(
            taken[g * heads : (g + 1) * heads], axis=0, keepdims=True
        ).astype(jnp.bfloat16)
    out_k.wait()
    out_v.wait()


def local(prompt, input_gain, key_weight, value_weight, key_gain, queries, score_bias):
    sp, tp = lax.axis_size("sp"), lax.axis_size("tp")
    seq_here, pos_here, width = prompt.shape
    cols = key_weight.shape[0]
    group = queries.shape[1]
    A = 2 ** (int(math.log2(tp)) // 2)
    B = tp // A
    halves = pos_here // LANES
    R = seq_here * halves
    length = pos_here * sp
    hbm, vmem = pl.BlockSpec(memory_space=pl.ANY), pl.BlockSpec(memory_space=pltpu.VMEM)
    dma = pltpu.SemaphoreType.DMA
    bf16 = jnp.bfloat16
    cache = pl.pallas_call(
        functools.partial(produce, (sp, tp, A, B, R, halves, cols, width)),
        out_shape=jax.ShapeDtypeStruct((2, cols, length), bf16),
        in_specs=[hbm, vmem, hbm, hbm, vmem],
        out_specs=hbm,
        scratch_shapes=[
            pltpu.VMEM((B * R, LANES, width), bf16),
            pltpu.VMEM((B * R, LANES, width), bf16),
            pltpu.VMEM((A, 2, cols, width), bf16),
            pltpu.VMEM((B * R, A, 2, cols, LANES), bf16),
            pltpu.VMEM((B * R, A - 1, 2, cols, LANES), bf16),
            pltpu.VMEM((HEAD, LANES), jnp.float32),
            dma((R,)),
            dma((2,)),
            dma(((B - 1) * R,)),
            dma(((B - 1) * R,)),
            dma((A - 1, W_CHUNKS)),
            dma((A - 1, W_CHUNKS)),
            dma((A - 1, W_CHUNKS)),
            dma((A - 1, W_CHUNKS)),
            dma((B * R, A - 1)),
            dma((B * R, A - 1)),
            dma((B * R * A,)),
            dma((sp * halves,)),
        ],
        compiler_params=pltpu.CompilerParams(
            collective_id=0, has_side_effects=True, vmem_limit_bytes=56 * 1024 * 1024
        ),
        name="produce",
    )(
        prompt.reshape(R, LANES, width),
        input_gain.reshape(1, width),
        key_weight,
        value_weight,
        key_gain.reshape(1, HEAD),
    )
    keys, values, first = pl.pallas_call(
        functools.partial(read, (group, cols // HEAD, cols, length)),
        out_shape=(
            jax.ShapeDtypeStruct((1, cols, length), bf16),
            jax.ShapeDtypeStruct((1, cols, length), bf16),
            jax.ShapeDtypeStruct((group, cols), bf16),
        ),
        in_specs=[vmem, vmem, hbm],
        out_specs=(hbm, hbm, vmem),
        scratch_shapes=[pltpu.VMEM((cols, length), bf16), pltpu.VMEM((cols, length), bf16), dma((4,))],
        name="read",
    )(queries.reshape(group, cols), score_bias, cache)
    return keys, values, first.reshape(1, group, cols)


def solution(mesh):
    placed = (P("tp", "sp", None), P(), P("tp", None), P("tp", None), P(), P("sp", None, "tp"), P())
    return jax.shard_map(
        local,
        mesh=mesh,
        in_specs=placed,
        out_specs=(P("sp", "tp", None), P("sp", "tp", None), P("sp", None, "tp")),
        check_vma=False,
    )
```

profile of v0, /device:TPU:3, one launch (start us, length us, event | category | flops | bytes accessed | tf_op | source)
XLA Modules:
  0.0 78.0 jit_solution(16075771355376056008)
XLA Ops:
  0.6 73.0 %produce.1.cache = bf16[2,256,2048]{2,1,0:T(8,128)(2,1)} custom-call(bf16[4,128,2048]{2,1,0:T(8,128)(2,1)} %bitcast.5, f32[1,2048]{1,0:T(1,128)} %bitcast.6, bf16[256,2048]{1,0:T(8,128)(2,1)} %key_w.1, bf16[256,2048]{1,0:T(8,128)(2,1)} %value_w.1, f32[1,64]{1,0:T(1,128)} %bitcast.8), custom_call_target="tpu_custom_call" | custom-call | tf_op jit(solution)/shard_map/produce/pallas_call | solution.py:331
  73.7 4.4 %read.1 = (bf16[1,256,2048]{2,1,0:T(8,128)(2,1)}, bf16[1,256,2048]{2,1,0:T(8,128)(2,1)}, bf16[2,256]{1,0:T(2,128)(2,1)}) custom-call(bf16[2,256]{1,0:T(2,128)(2,1)} %bitcast.7, f32[2,16]{1,0:T(2,128)} %bias.1, bf16[2,256,2048]{2,1,0:T(8,128)(2,1)} %produce.1.cache), custom_call_target="tpu_custom_call" | custom-call | tf_op jit(solution)/shard_map/read/pallas_call | solution.py:367
where the time goes:
time: 78.2 us; the launch traced here: 78 us
  Pallas kernels  77.4 us (99%)
    pallas_call x1, Pallas kernels, local(): pl.pallas_call(functools.partial(produce, (sp, tp, A, B, R, halves, cols,...  73 us
    pallas_call x1, Pallas kernels, local(): pl.pallas_call(functools.partial(read, (group, cols // HEAD, cols, length...  4.35 us

commit v1 on v0

--- a/solution.py
+++ b/solution.py
@@ -104,14 +104,11 @@
             send_x(db, i).start()
 
     def normalise(r):
-        def rows(k, _):
-            here = pl.ds(pl.multiple_of(k * NORM_ROWS, NORM_ROWS), NORM_ROWS)
+        for k in range(LANES // NORM_ROWS):
+            here = pl.ds(k * NORM_ROWS, NORM_ROWS)
             flat = x[r, here, :].astype(jnp.float32)
             scale = lax.rsqrt(jnp.mean(flat * flat, axis=-1, keepdims=True) + epsilon)
             xn[r, here, :] = (flat * scale * gain[...]).astype(jnp.bfloat16)
-            return 0
-
-        lax.fori_loop(0, LANES // NORM_ROWS, rows, 0)
 
     eye = lax.broadcasted_iota(jnp.int32, (HEAD, HEAD), 0) == lax.broadcasted_iota(jnp.int32, (HEAD, HEAD), 1)
     gain_column[...] = jnp.broadcast_to(
@@ -138,7 +135,7 @@
         def start(self):
             @pl.when(self.here)
             def _():
-                pltpu.make_async_copy(self.block, self.place, self.sem).start()
+                self.place[...] = self.block[...]
 
             @pl.when(jnp.logical_not(self.here))
             def _():
@@ -251,24 +248,29 @@
             if da:
                 hop(r, da).wait_send()
 
-    def landed(n, _):
+    def arrived(n):
         place = cache.at[:, :, pl.ds(pl.multiple_of(n * LANES, LANES), LANES)]
         pltpu.make_async_copy(out.at[0, 0], place, o_recv.at[n]).wait()
+
+    def landed(n, _):
+        @pl.when(n // halves != s)
+        def _():
+            arrived(n)
+
         return 0
 
     lax.fori_loop(0, sp * halves, landed, 0)
 
 
-def read(dims, queries, bias, cache, keys_out, values_out, first_out, keys, values, sems):
+def read(dims, queries, bias, cache, keys_out, values_out, first_out, sems):
     group, heads, cols, length = dims
     rows = group * heads
     t = lax.axis_index("tp")
-    in_k = pltpu.make_async_copy(cache.at[0], keys, sems.at[0])
-    in_v = pltpu.make_async_copy(cache.at[1], values, sems.at[1])
+    keys, values = cache.at[0], cache.at[1]
     out_k = pltpu.make_async_copy(keys, keys_out.at[0], sems.at[2])
     out_v = pltpu.make_async_copy(values, values_out.at[0], sems.at[3])
-    in_k.start()
-    in_v.start()
+    out_k.start()
+    out_v.start()
 
     def spread(ref_value):
         n = ref_value.shape[1]
@@ -283,8 +285,6 @@
     mine = at == t * heads + lax.broadcasted_iota(jnp.int32, offsets.shape, 0) % heads
     offset = jnp.sum(jnp.where(mine, offsets, 0.0), axis=1, keepdims=True)
 
-    in_k.wait()
-    out_k.start()
     scores = jnp.dot(query, keys[...], preferred_element_type=jnp.float32)
     scores = scores / math.sqrt(HEAD) + offset
     soft = jnp.log1p(jnp.exp(-jnp.abs(scores)))
@@ -301,8 +301,6 @@
         later = later + ahead(later, k)
         k *= 2
     weights = jnp.exp(log_break + later).astype(jnp.bfloat16)
-    in_v.wait()
-    out_v.start()
     taken = lax.dot_general(
         weights, values[...], (((1,), (1,)), ((), ())), preferred_element_type=jnp.float32
     )
@@ -330,9 +328,9 @@
     bf16 = jnp.bfloat16
     cache = pl.pallas_call(
         functools.partial(produce, (sp, tp, A, B, R, halves, cols, width)),
-        out_shape=jax.ShapeDtypeStruct((2, cols, length), bf16),
+        out_shape=pltpu.VMEM((2, cols, length), bf16),
         in_specs=[hbm, vmem, hbm, hbm, vmem],
-        out_specs=hbm,
+        out_specs=vmem,
         scratch_shapes=[
             pltpu.VMEM((B * R, LANES, width), bf16),
             pltpu.VMEM((B * R, LANES, width), bf16),
@@ -364,6 +362,7 @@
         value_weight,
         key_gain.reshape(1, HEAD),
     )
+    cache = pltpu.with_memory_space_constraint(cache, pltpu.VMEM)
     keys, values, first = pl.pallas_call(
         functools.partial(read, (group, cols // HEAD, cols, length)),
         out_shape=(
@@ -371,9 +370,9 @@
             jax.ShapeDtypeStruct((1, cols, length), bf16),
             jax.ShapeDtypeStruct((group, cols), bf16),
         ),
-        in_specs=[vmem, vmem, hbm],
+        in_specs=[vmem, vmem, vmem],
         out_specs=(hbm, hbm, vmem),
-        scratch_shapes=[pltpu.VMEM((cols, length), bf16), pltpu.VMEM((cols, length), bf16), dma((4,))],
+        scratch_shapes=[dma((4,))],
         name="read",
     )(queries.reshape(group, cols), score_bias, cache)
     return keys, values, first.reshape(1, group, cols)

time: 78.2 us -> 77.6 us (level)
    pallas_call x1, Pallas kernels: 4.35 us -> 3.04 us  [local(): pl.pallas_call(functools.partial(read, (group, cols // HEAD, cols, length...]
where the time goes in v1:
time: 77.6 us; the launch traced here: 77.3 us
  Pallas kernels  76.7 us (99%)
    pallas_call x1, Pallas kernels, local(): pl.pallas_call(functools.partial(produce, (sp, tp, A, B, R, halves, cols,...  73.6 us
    pallas_call x1, Pallas kernels, local(): pl.pallas_call(functools.partial(read, (group, cols // HEAD, cols, length...  3.04 us

profile of v1, /device:TPU:3, one launch (start us, length us, event | category | flops | bytes accessed | tf_op | source)
XLA Modules:
  0.0 77.3 jit_solution(12846455527340107432)
XLA Ops:
  0.6 73.6 %produce.1.cache = bf16[2,256,2048]{2,1,0:T(8,128)(2,1)S(1)} custom-call(bf16[4,128,2048]{2,1,0:T(8,128)(2,1)} %bitcast.5, f32[1,2048]{1,0:T(1,128)} %bitcast.6, bf16[256,2048]{1,0:T(8,128)(2,1)} %key_w.1, bf16[256,2048]{1,0:T(8,128)(2,1)} %value_w.1, f32[1,64]{1,0:T(1,128)} %bitcast.8), custom_call_target="tpu_custom_call" | custom-call | tf_op jit(solution)/shard_map/produce/pallas_call | solution.py:329
  74.3 3.0 %read.1 = (bf16[1,256,2048]{2,1,0:T(8,128)(2,1)}, bf16[1,256,2048]{2,1,0:T(8,128)(2,1)}, bf16[2,256]{1,0:T(2,128)(2,1)}) custom-call(bf16[2,256]{1,0:T(2,128)(2,1)} %bitcast.7, f32[2,16]{1,0:T(2,128)} %bias.1, bf16[2,256,2048]{2,1,0:T(8,128)(2,1)S(1)} %produce.1.cache), custom_call_target="tpu_custom_call" | custom-call | tf_op jit(solution)/shard_map/read/pallas_call | solution.py:366

commit v2 on v1

--- a/solution.py
+++ b/solution.py
@@ -212,10 +212,10 @@
         for da in range(1, A):
             arrived_w(da, k).wait_recv()
 
-    order = []
-    for n in range(max(early, R)):
-        order += theirs[n : n + 1] if n < early else []
-        order += [n] if n < R else []
+    stays = (2 * t * seqs >= sp) == (2 * s >= sp)
+    others_first = theirs[:early] + list(range(R))
+    own_first_order = list(range(R)) + theirs[:early]
+    order = [jnp.where(stays, a, b) for a, b in zip(others_first, own_first_order)]
     order += theirs[early:]
     given, passed = 0, 0
     for r in order[: early + R]:
@@ -227,7 +227,7 @@
     for n in range(early, N):
         give(take(n))
         given += 1
-        while passed < min(R + 2 * (n - early + 1), given if n == N - 1 else given - 1):
+        while passed < (given if n == N - 1 else given - 1):
             pass_on(order[passed])
             passed += 1
     while passed < len(order):

time: 77.6 us -> 75.9 us (0.978); the launches traced: 77.3 us -> 74.5 us
  Pallas kernels: 76.7 us -> 73.9 us
    pallas_call x1, Pallas kernels: 73.6 us -> 70.8 us  [local(): pl.pallas_call(functools.partial(produce, (sp, tp, A, B, R, halves, cols,...]
where the time goes in v2:
time: 75.9 us; the launch traced here: 74.5 us
  Pallas kernels  73.9 us (97%)
    pallas_call x1, Pallas kernels, local(): pl.pallas_call(functools.partial(produce, (sp, tp, A, B, R, halves, cols,...  70.8 us
    pallas_call x1, Pallas kernels, local(): pl.pallas_call(functools.partial(read, (group, cols // HEAD, cols, length...  3.04 us

profile of v2, /device:TPU:3, one launch (start us, length us, event | category | flops | bytes accessed | tf_op | source)
XLA Modules:
  0.0 74.5 jit_solution(2041688626873931872)
XLA Ops:
  0.6 70.8 %produce.1.cache = bf16[2,256,2048]{2,1,0:T(8,128)(2,1)S(1)} custom-call(bf16[4,128,2048]{2,1,0:T(8,128)(2,1)} %bitcast.5, f32[1,2048]{1,0:T(1,128)} %bitcast.6, bf16[256,2048]{1,0:T(8,128)(2,1)} %key_w.1, bf16[256,2048]{1,0:T(8,128)(2,1)} %value_w.1, f32[1,64]{1,0:T(1,128)} %bitcast.8), custom_call_target="tpu_custom_call" | custom-call | tf_op jit(solution)/shard_map/produce/pallas_call | solution.py:329
  71.5 3.0 %read.1 = (bf16[1,256,2048]{2,1,0:T(8,128)(2,1)}, bf16[1,256,2048]{2,1,0:T(8,128)(2,1)}, bf16[2,256]{1,0:T(2,128)(2,1)}) custom-call(bf16[2,256]{1,0:T(2,128)(2,1)} %bitcast.7, f32[2,16]{1,0:T(2,128)} %bias.1, bf16[2,256,2048]{2,1,0:T(8,128)(2,1)S(1)} %produce.1.cache), custom_call_target="tpu_custom_call" | custom-call | tf_op jit(solution)/shard_map/read/pallas_call | solution.py:366

commit v3 on v2

--- a/solution.py
+++ b/solution.py
@@ -298,8 +298,12 @@
     later = ahead(log_keep, 1)
     k = 1
     while k < length:
-        later = later + ahead(later, k)
-        k *= 2
+        if 4 * k <= length:
+            later = (later + ahead(later, k)) + (ahead(later, 2 * k) + ahead(later, 3 * k))
+            k *= 4
+        else:
+            later = later + ahead(later, k)
+            k *= 2
     weights = jnp.exp(log_break + later).astype(jnp.bfloat16)
     taken = lax.dot_general(
         weights, values[...], (((1,), (1,)), ((), ())), preferred_element_type=jnp.float32

time: 75.9 us -> 75.5 us (level)
  no operation moved by 1% of the time
where the time goes in v3:
time: 75.5 us; the launch traced here: 74.1 us
  Pallas kernels  73.5 us (97%)
    pallas_call x1, Pallas kernels, local(): pl.pallas_call(functools.partial(produce, (sp, tp, A, B, R, halves, cols,...  70.8 us
    pallas_call x1, Pallas kernels, local(): pl.pallas_call(functools.partial(read, (group, cols // HEAD, cols, length...  2.62 us

profile of v3, /device:TPU:3, one launch (start us, length us, event | category | flops | bytes accessed | tf_op | source)
XLA Modules:
  0.0 74.1 jit_solution(13971399211294435218)
XLA Ops:
  0.6 70.8 %produce.1.cache = bf16[2,256,2048]{2,1,0:T(8,128)(2,1)S(1)} custom-call(bf16[4,128,2048]{2,1,0:T(8,128)(2,1)} %bitcast.5, f32[1,2048]{1,0:T(1,128)} %bitcast.6, bf16[256,2048]{1,0:T(8,128)(2,1)} %key_w.1, bf16[256,2048]{1,0:T(8,128)(2,1)} %value_w.1, f32[1,64]{1,0:T(1,128)} %bitcast.8), custom_call_target="tpu_custom_call" | custom-call | tf_op jit(solution)/shard_map/produce/pallas_call | solution.py:333
  71.5 2.6 %read.1 = (bf16[1,256,2048]{2,1,0:T(8,128)(2,1)}, bf16[1,256,2048]{2,1,0:T(8,128)(2,1)}, bf16[2,256]{1,0:T(2,128)(2,1)}) custom-call(bf16[2,256]{1,0:T(2,128)(2,1)} %bitcast.7, f32[2,16]{1,0:T(2,128)} %bias.1, bf16[2,256,2048]{2,1,0:T(8,128)(2,1)S(1)} %produce.1.cache), custom_call_target="tpu_custom_call" | custom-call | tf_op jit(solution)/shard_map/read/pallas_call | solution.py:370
